TPU v7x, 32 devices: a whole 2x2x4 slice. The times are simulated.
32 devices in a mesh: sp: 8 (over z, x), dp: 4 (over y, core).
Axes of the slice: x: 2, y: 2, z: 4, core: 2. Of those that a mesh axis runs over, the one named last changes fastest.
Arguments:
- tokens: bfloat16 [4, 4096, 2048], P('dp', 'sp'), may hold values from -6 to 6
- segments: int32 [4, 4096], P('dp', 'sp'), may hold values from 0 to 3, never falling along the last dimension, each value on 1 to 2048 neighbouring positions
- w_lin: bfloat16 [2048, 1024], P('dp'), may hold values from -0.125 to 0.125
- w_gate: bfloat16 [2048, 1024], P('dp'), may hold values from -0.125 to 0.125
- w_out: bfloat16 [1024, 2048], P(None, 'dp'), may hold values from -0.1875 to 0.1875
- conv_kernel: float32 [31, 1024], replicated, may hold values from -1 to 1
- conv_bias: float32 [1024], replicated, may hold values from -3 to 3
- norm_gain: float32 [1024], replicated, may hold values from 0.1 to 1.9
- norm_bias: float32 [1024], replicated, may hold values from -3 to 3
Outputs:
- mixed_out: bfloat16 [4, 4096, 2048], P('dp', 'sp')
Inputs may be any that keep to these rules, and one draw needn't show every extreme that they name: `segments`: within each sequence document numbers never fall; a document is a run of equal numbers of at most four times 512 positions.
All inputs are finite; a program needn't handle non-finite values.
Results may differ from a plain program's by a relative error of at most 0.0062.
Values may be sent and summed in bfloat16 or wider, within the bound.
No kernel may reach another device: no remote copies, remote signals or barrier semaphores. Data moves between devices by JAX's collectives and lax.ppermute only.
A program may use at most 64 MiB of HBM per device.

v0:
```python
import jax
import jax.numpy as jnp
from jax import lax
from jax.sharding import PartitionSpec as P

K = 31


def from_behind(value, axis, by):
    devices = lax.axis_size(axis)
    pairs = [(i, i + by) for i in range(devices) if 0 <= i + by < devices]
    return lax.ppermute(value, axis, pairs)


def conv_doc(values, doc_ids, kernel, bias):
    taps = kernel.shape[0]
    reach = taps - 1
    length = values.shape[1]
    place = lax.iota(jnp.int32, length)
    change = jnp.concatenate([jnp.ones((1,), jnp.bool_), doc_ids[1:] != doc_ids[:-1]])
    begins = lax.cummax(jnp.where(change, place, 0), axis=0)[reach:]
    here = place[reach:]
    total = bias[:, None] + kernel[reach][:, None] * values[:, reach:].astype(jnp.float32)
    for back in range(1, taps):
        piece = values[:, reach - back : length - back].astype(jnp.float32)
        keep = here - back >= begins
        total = total + kernel[reach - back][:, None] * jnp.where(keep[None, :], piece, 0.0)
    return total


def body(tokens, segments, w_lin, w_gate, w_out, conv_kernel, conv_bias, norm_gain, norm_bias):
    rows = tokens[0]
    doc_ids = segments[0]
    count = rows.shape[0]
    reach = K - 1
    first = jnp.einsum(
        "rc,tr->ct",
        lax.all_gather(w_lin, "dp", axis=0, tiled=True),
        rows,
        preferred_element_type=jnp.float32,
    )
    second = jnp.einsum(
        "rc,tr->ct",
        lax.all_gather(w_gate, "dp", axis=0, tiled=True),
        rows,
        preferred_element_type=jnp.float32,
    )
    glu = (first * jax.nn.sigmoid(second)).astype(jnp.bfloat16)
    tail, tail_ids = from_behind((glu[:, count - reach :], doc_ids[count - reach :]), "sp", 1)
    extended = jnp.concatenate([tail, glu], axis=1)
    ext_ids = jnp.concatenate([tail_ids, doc_ids], axis=0)
    conv = conv_doc(extended, ext_ids, conv_kernel, conv_bias)
    conved = lax.optimization_barrier(conv.astype(jnp.bfloat16))
    values = conved.astype(jnp.float32)
    mean = jnp.mean(values, axis=0, keepdims=True)
    var = jnp.mean(jnp.square(values - mean), axis=0, keepdims=True)
    normed = (values - mean) * lax.rsqrt(var + 1e-05) * norm_gain[:, None] + norm_bias[:, None]
    act = jax.nn.silu(normed).astype(jnp.bfloat16)
    mixed_out = jnp.einsum(
        "ct,cr->tr",
        act,
        lax.all_gather(w_out, "dp", axis=1, tiled=True),
        preferred_element_type=jnp.float32,
    ).astype(jnp.bfloat16)
    return mixed_out[None]


def solution(mesh):
    placed = (
        P("dp", "sp", None),
        P("dp", "sp"),
        P("dp", None),
        P("dp", None),
        P(None, "dp"),
        P(),
        P(),
        P(),
        P(),
    )
    return jax.shard_map(
        body, mesh=mesh, in_specs=placed, out_specs=P("dp", "sp", None), check_vma=False
    )
```

profile of v0, /device:TPU:0, one launch (start us, length us, event | category | flops | bytes accessed | tf_op | source)
XLA Modules:
  0.0 131.1 jit_solution(17335974425128062268)
XLA Ops:
  6.5 0.0 copy-start
  6.5 0.0 copy-start.3
  6.5 0.0 copy-start.1
  6.5 0.0 all-gather.4.cloned.1.call-start
  6.5 0.7 all-gather.4.cloned.1.call-update
  7.3 0.0 all-gather.6.cloned.1.call-start
  7.3 0.7 all-gather.6.cloned.1.call-update
  8.0 0.0 all-gather.8.cloned.1.call-start
  8.1 0.0 copy-done.3
  8.1 0.1 slice_bitcast_fusion
  8.1 4.9 %collective-permute-start = (s32[30]{0:T(128)S(1)}, s32[30]{0:T(128)S(1)}, u32[]{:S(2)}, u32[]{:S(2)}) collective-permute-start(s32[30]{0:T(128)S(1)} %slice_bitcast_fusion), channel_id=1, source_target_pairs={{0,4},{4,8},{8,12},{12,16},{16,20},{20,24},{24,28},{1,5},{5,9},{9,... | collective-permute-start | bytes 368 | tf_op jit(solution)/shard_map/ppermute | solution.py:12
  13.0 0.0 all-gather.8.cloned.1.call-update
  13.0 0.0 copy-done.1
  13.0 0.1 fusion.54
  13.2 1.1 collective-permute-done
  14.3 0.1 pad_add_fusion
  14.4 0.1 slice_compare_fusion
  14.4 0.1 iota_select_fusion
  14.5 0.3 reduce-window.9
  14.8 0.1 slice.278
  14.9 0.1 slice_reduce_fusion
  15.0 0.1 maximum_bitcast_fusion
  15.1 0.1 add_compare_fusion.20
  15.2 0.1 add_compare_fusion.11
  15.3 0.1 add_compare_fusion.29
  15.3 30.8 %all-gather.4.cloned.1.call-done = bf16[2048,1024]{1,0:T(8,128)(2,1)} async-done(((bf16[512,1024]{1,0:T(8,128)(2,1)}), bf16[2048,1024]{1,0:T(8,128)(2,1)}) %all-gather.4.cloned.1.call-update) | async-done | bytes 4194320 | tf_op jit(solution)/shard_map/all_gather | solution.py:38
  46.1 0.0 copy-done
  46.1 5.8 %fusion.12 = f32[1024,512]{0,1:T(8,128)} fusion(bf16[2048,1024]{1,0:T(8,128)(2,1)} %all-gather.4.cloned.1.call-done, bf16[1,512,2048]{2,1,0:T(8,128)(2,1)S(1)} %copy-done), kind=kOutput, calls=%fused_computation.44 | convolution fusion | flops 2147483648 | bytes 8388608 | tf_op jit(solution)/shard_map/rc,tr->ct/dot_general | solution.py:36
  52.0 0.0 copy-start.2
  52.0 30.2 %all-gather.6.cloned.1.call-done = bf16[2048,1024]{1,0:T(8,128)(2,1)} async-done(((bf16[512,1024]{1,0:T(8,128)(2,1)}), bf16[2048,1024]{1,0:T(8,128)(2,1)}) %all-gather.6.cloned.1.call-update) | async-done | bytes 4194320 | tf_op jit(solution)/shard_map/all_gather | solution.py:44
  82.2 5.4 %multiply_convert_fusion = bf16[1024,512]{0,1:T(8,128)(2,1)S(1)} fusion(f32[1024,512]{0,1:T(8,128)} %fusion.12, bf16[2048,1024]{1,0:T(8,128)(2,1)} %all-gather.6.cloned.1.call-done, bf16[1,512,2048]{2,1,0:T(8,128)(2,1)S(1)} %copy-done), kind=kOutput, calls=%fused_computation.49 | convolution fusion | flops 2150105088 | bytes 9437184 | tf_op jit(solution)/shard_map/rc,tr->ct/dot_general | solution.py:42
  87.6 3.4 %collective-permute-start.1 = (bf16[1024,30]{0,1:T(8,128)(2,1)S(1)}, bf16[1024,30]{0,1:T(8,128)(2,1)S(1)}, u32[]{:S(2)}, u32[]{:S(2)}) collective-permute-start(bf16[1024,30]{0,1:T(8,128)(2,1)S(1)} %slice.341), channel_id=1, source_target_pairs={{0,4},{4,8},{8,12},{12,16},{16,20},{20,24},{24,28},{1,5},{5,9},{9,... | collective-permute-start | bytes 184328 | tf_op jit(solution)/shard_map/ppermute | solution.py:12
  91.0 0.1 add_compare_fusion.2
  91.1 1.8 %collective-permute-done.1 = bf16[1024,30]{0,1:T(8,128)(2,1)S(1)} collective-permute-done((bf16[1024,30]{0,1:T(8,128)(2,1)S(1)}, bf16[1024,30]{0,1:T(8,128)(2,1)S(1)}, u32[]{:S(2)}, u32[]{:S(2)}) %collective-permute-start.1) | collective-permute-done | bytes 61472 | tf_op jit(solution)/shard_map/ppermute | solution.py:12
  92.9 0.0 copy-done.2
  92.9 0.0 copy-start.4
  92.9 0.0 copy-start.5
  92.9 15.9 %add_convert_fusion = bf16[1024,512]{0,1:T(8,128)(2,1)S(1)} fusion(bf16[1024,512]{0,1:T(8,128)(2,1)S(1)} %multiply_convert_fusion, bf16[1024,30]{0,1:T(8,128)(2,1)S(1)} %collective-permute-done.1, f32[1024]{0:T(1024)S(1)} %bitcast.79, f32[1024]{0:T(1024)S(1)} %bitcast.80, f32[1024]{0:T(1024)S(1)} %bitcast.51, f32[1024]{0:T(1024)S(1)} %bitcast.52, ...), kind=kLoop, calls=%fused_computation.48 | loop fusion | flops 112197632 | bytes 2305024 | tf_op jit(solution)/shard_map/convert_element_type | solution.py:53
  108.8 0.2 convert_reduce_fusion
  109.0 0.4 fusion.3
  109.5 8.8 %all-gather.8.cloned.1.call-done = bf16[1024,2048]{1,0:T(8,128)(2,1)} async-done(((bf16[1024,512]{1,0:T(8,128)(2,1)}), bf16[1024,2048]{1,0:T(8,128)(2,1)}) %all-gather.8.cloned.1.call-update) | async-done | bytes 4194320 | tf_op jit(solution)/shard_map/all_gather | solution.py:62
  118.2 0.0 copy-done.4
  118.2 0.0 copy-done.5
  118.2 6.3 %fusion = bf16[1,512,2048]{2,1,0:T(8,128)(2,1)} fusion(bf16[1024,2048]{1,0:T(8,128)(2,1)} %all-gather.8.cloned.1.call-done, bf16[1024,512]{0,1:T(8,128)(2,1)S(1)} %add_convert_fusion, f32[1024]{0:T(1024)S(1)} %copy-done.4, f32[1024]{0:T(1024)S(1)} %copy-done.5, f32[512]{0:T(512)S(1)} %add_rsqrt_fusion, f32[512]{0:T(512)S(1)} %broadcast_multiply_fusion), kind=kOutput, calls=%fused_computation.30 | convolution fusion | flops 2153775104 | bytes 7352320 | tf_op jit(solution)/shard_map/ct,cr->tr/dot_general | solution.py:59
  (7 shorter events, 0.1 us)
Async XLA Ops:
  6.5 39.6 %copy-start = (bf16[1,512,2048]{2,1,0:T(8,128)(2,1)S(1)}, bf16[1,512,2048]{2,1,0:T(8,128)(2,1)}, u32[]{:S(2)}) copy-start(bf16[1,512,2048]{2,1,0:T(8,128)(2,1)} %param.9) | copy-start | bytes 6291460
  6.5 1.5 %copy-start.3 = (s32[1,512]{1,0:T(1,128)S(1)}, s32[1,512]{1,0:T(1,128)}, u32[]{:S(2)}) copy-start(s32[1,512]{1,0:T(1,128)} %param.10) | copy-start | bytes 6148
  6.5 6.5 %copy-start.1 = (f32[31,1024]{1,0:T(8,128)S(1)}, f32[31,1024]{1,0:T(8,128)}, u32[]{:S(2)}) copy-start(f32[31,1024]{1,0:T(8,128)} %param.14) | copy-start | bytes 380932
  6.5 39.6 %all-gather.4.cloned.1.call-start = ((), (), s32[]{:S(2)}) async-start(), calls=%async_computation | async-start | bytes 5242880 | tf_op jit(solution)/shard_map/all_gather | solution.py:38
  7.3 74.9 %all-gather.6.cloned.1.call-start = ((), (), s32[]{:S(2)}) async-start(), calls=%async_computation.1 | async-start | bytes 5242880 | tf_op jit(solution)/shard_map/all_gather | solution.py:44
  8.0 110.2 %all-gather.8.cloned.1.call-start = ((), (), s32[]{:S(2)}) async-start(), calls=%async_computation.2 | async-start | bytes 5242880 | tf_op jit(solution)/shard_map/all_gather | solution.py:62
  8.1 6.1 %collective-permute-start = (s32[30]{0:T(128)S(1)}, s32[30]{0:T(128)S(1)}, u32[]{:S(2)}, u32[]{:S(2)}) collective-permute-start(s32[30]{0:T(128)S(1)} %slice_bitcast_fusion), channel_id=1, source_target_pairs={{0,4},{4,8},{8,12},{12,16},{16,20},{20,24},{24,28},{1,5},{5,9},{9,... | collective-permute-start | bytes 368 | tf_op jit(solution)/shard_map/ppermute | solution.py:12
  52.0 40.9 %copy-start.2 = (f32[1024]{0:T(1024)S(1)}, f32[1024]{0:T(1024)}, u32[]{:S(2)}) copy-start(f32[1024]{0:T(1024)} %param.15) | copy-start | bytes 12292
  87.6 5.3 %collective-permute-start.1 = (bf16[1024,30]{0,1:T(8,128)(2,1)S(1)}, bf16[1024,30]{0,1:T(8,128)(2,1)S(1)}, u32[]{:S(2)}, u32[]{:S(2)}) collective-permute-start(bf16[1024,30]{0,1:T(8,128)(2,1)S(1)} %slice.341), channel_id=1, source_target_pairs={{0,4},{4,8},{8,12},{12,16},{16,20},{20,24},{24,28},{1,5},{5,9},{9,... | collective-permute-start | bytes 184328 | tf_op jit(solution)/shard_map/ppermute | solution.py:12
  92.9 25.3 %copy-start.4 = (f32[1024]{0:T(1024)S(1)}, f32[1024]{0:T(1024)}, u32[]{:S(2)}) copy-start(f32[1024]{0:T(1024)} %param.17) | copy-start | bytes 12292
  92.9 25.3 %copy-start.5 = (f32[1024]{0:T(1024)S(1)}, f32[1024]{0:T(1024)}, u32[]{:S(2)}) copy-start(f32[1024]{0:T(1024)} %param.16) | copy-start | bytes 12292
Sparse Core Ops, SparseCore 0:
  8.9 37.1 all-gather.3
  47.7 34.4 all-gather.5
  83.7 34.4 all-gather.7
where the time goes:
time: 131 us
  waiting for transfers between devices  74.1 us (57%)
  matrix products  17.6 us (13%)
  other arithmetic  17.5 us (13%)
  between operations  13.2 us (10%)
  starting transfers between devices  8.31 us (6%)
    all_gather x1, waiting for transfers between devices, body(): lax.all_gather(w_lin, 'dp', axis=0, tiled=True)  30.8 us
    all_gather x1, waiting for transfers between devices, body(): lax.all_gather(w_gate, 'dp', axis=0, tiled=True)  30.2 us
    convert_element_type x1, other arithmetic, body(): conved = lax.optimization_barrier(conv.astype(jnp.bfloat16))  15.9 us
    all_gather x1, waiting for transfers between devices, body(): lax.all_gather(w_out, 'dp', axis=1, tiled=True)  8.75 us
    ppermute x2, starting transfers between devices, from_behind(): return lax.ppermute(value, axis, pairs)  8.23 us
    dot_general x1, matrix products, body(): jnp.einsum('ct,cr->tr', act, lax.all_gather(w_out, 'dp', axis=1, tiled=Tr...  6.35 us
    dot_general x1, matrix products, body(): jnp.einsum('rc,tr->ct', lax.all_gather(w_lin, 'dp', axis=0, tiled=True),...  5.84 us
    dot_general x1, matrix products, body(): jnp.einsum('rc,tr->ct', lax.all_gather(w_gate, 'dp', axis=0, tiled=True),...  5.44 us
  transfers between devices with their start and end apart: 5, of which 5 were waited for; matrix products, arithmetic and copies ran while one was open for 22% of the time, Pallas kernels for 0%

commit v1 on v0

--- a/solution.py
+++ b/solution.py
@@ -33,12 +33,27 @@
     doc_ids = segments[0]
     count = rows.shape[0]
     reach = K - 1
-    first = jnp.einsum(
+    count_2, mine = (lax.axis_size("dp"), lax.axis_index("dp"))
+    left = [(i_2, (i_2 - 1) % count_2) for i_2 in range(count_2)]
+    rows_2 = w_lin.shape[0]
+    block = w_lin
+    total_2 = jnp.einsum(
         "rc,tr->ct",
-        lax.all_gather(w_lin, "dp", axis=0, tiled=True),
-        rows,
+        block,
+        lax.dynamic_slice_in_dim(rows, mine * rows_2, block.shape[0], axis=1),
         preferred_element_type=jnp.float32,
     )
+    for step in range(1, count_2):
+        block = lax.ppermute(block, "dp", left)
+        total_2 = total_2 + jnp.einsum(
+            "rc,tr->ct",
+            block,
+            lax.dynamic_slice_in_dim(
+                rows, (mine + step) % count_2 * rows_2, block.shape[0], axis=1
+            ),
+            preferred_element_type=jnp.float32,
+        )
+    first = total_2
     second = jnp.einsum(
         "rc,tr->ct",
         lax.all_gather(w_gate, "dp", axis=0, tiled=True),

time: 131 us -> 118 us (0.901); the launches traced: 131 us -> 117 us
  waiting for transfers between devices: 74.1 us -> 50.5 us
  starting transfers between devices: 8.31 us -> 12.8 us
  matrix products: 17.6 us -> 21.2 us
    ppermute x0 -> x3, waiting for transfers between devices: none -> 48 us  [body(): block = lax.ppermute(block, 'dp', left)]
    all_gather x1 -> x0, waiting for transfers between devices: 30.8 us -> none  [body(): lax.all_gather(w_lin, 'dp', axis=0, tiled=True)]
    all_gather x1, waiting for transfers between devices: 30.2 us -> 0.01 us  [body(): lax.all_gather(w_gate, 'dp', axis=0, tiled=True)]
    all_gather x1, waiting for transfers between devices: 8.75 us -> 0.02 us  [body(): lax.all_gather(w_out, 'dp', axis=1, tiled=True)]
    ppermute x0 -> x3, starting transfers between devices: none -> 6.49 us  [body(): block = lax.ppermute(block, 'dp', left)]
    dot_general x1 -> x4, matrix products: 5.84 us -> 9.69 us  [the longest x3 7.59 us: body(): jnp.einsum('rc,tr->ct', block, lax.dynamic_slice_in_dim(rows, (mine + ste...]
    ppermute x2, starting transfers between devices: 8.23 us -> 6.32 us  [from_behind(): return lax.ppermute(value, axis, pairs)]
  transfers between devices with their start and end apart: 5 -> 7, of which waited for: 5 -> 4; matrix products, arithmetic and copies ran while one was open for 22% -> 29% of each run, Pallas kernels for 0% -> 0%
where the time goes in v1:
time: 118 us; the launch traced here: 117 us
  waiting for transfers between devices  50.5 us (43%)
  matrix products  21.2 us (18%)
  other arithmetic  17.5 us (15%)
  between operations  13.6 us (12%)
  starting transfers between devices  12.8 us (11%)
    ppermute x3, waiting for transfers between devices, body(): block = lax.ppermute(block, 'dp', left)  48 us
    convert_element_type x1, other arithmetic, body(): conved = lax.optimization_barrier(conv.astype(jnp.bfloat16))  15.9 us
    dot_general x3, matrix products, body(): jnp.einsum('rc,tr->ct', block, lax.dynamic_slice_in_dim(rows, (mine + ste...  7.59 us
    ppermute x3, starting transfers between devices, body(): block = lax.ppermute(block, 'dp', left)  6.49 us
    dot_general x1, matrix products, body(): jnp.einsum('ct,cr->tr', act, lax.all_gather(w_out, 'dp', axis=1, tiled=Tr...  6.34 us
    ppermute x2, starting transfers between devices, from_behind(): return lax.ppermute(value, axis, pairs)  6.32 us
    dot_general x1, matrix products, body(): jnp.einsum('rc,tr->ct', lax.all_gather(w_gate, 'dp', axis=0, tiled=True),...  5.13 us
  transfers between devices with their start and end apart: 7, of which 4 were waited for; matrix products, arithmetic and copies ran while one was open for 29% of the time, Pallas kernels for 0%

profile of v1, /device:TPU:0, one launch (start us, length us, event | category | flops | bytes accessed | tf_op | source)
XLA Modules:
  0.0 116.7 jit_solution(3166367386002997402)
XLA Ops:
  6.5 0.0 copy-start
  6.5 0.0 all-gather.3.cloned.1.call-start
  6.5 0.7 all-gather.3.cloned.1.call-update
  7.3 0.0 all-gather.5.cloned.1.call-start
  7.3 2.5 %collective-permute-start = (bf16[512,1024]{1,0:T(8,128)(2,1)}, bf16[512,1024]{1,0:T(8,128)(2,1)}, u32[]{:S(2)}, u32[]{:S(2)}) collective-permute-start(bf16[512,1024]{1,0:T(8,128)(2,1)} %param.11), channel_id=1, source_target_pairs={{0,3},{1,0},{2,1},{3,2},{4,7},{5,4},{6,5},{7,6},{8,11},{9,8},{10,9... | collective-permute-start | bytes 3145736 | tf_op jit(solution)/shard_map/ppermute | solution.py:47
  9.8 0.7 slice_bitcast_fusion
  10.5 3.4 %collective-permute-start.3 = (s32[30]{0:T(128)S(1)}, s32[30]{0:T(128)S(1)}, u32[]{:S(2)}, u32[]{:S(2)}) collective-permute-start(s32[30]{0:T(128)S(1)} %slice_bitcast_fusion), channel_id=1, source_target_pairs={{0,4},{4,8},{8,12},{12,16},{16,20},{20,24},{24,28},{1,5},{5,9},{9,... | collective-permute-start | bytes 368 | tf_op jit(solution)/shard_map/ppermute | solution.py:12
  13.9 0.0 all-gather.5.cloned.1.call-update
  13.9 0.0 copy-done.5
  13.9 0.0 copy-start.7
  14.1 0.1 fusion.66
  14.1 0.0 copy-done
  14.1 0.0 copy-done.4
  14.1 2.1 %fusion.55 = f32[512,1024]{1,0:T(8,128)} fusion(bf16[512,1024]{1,0:T(8,128)(2,1)S(1)} %copy-done.4, bf16[1,512,2048]{2,1,0:T(8,128)(2,1)S(1)} %copy-done, s32[]{:T(128)S(6)} %select_n.122), kind=kOutput, calls=%fused_computation.94 | convolution fusion | flops 536870912 | bytes 3670020 | tf_op jit(solution)/shard_map/rc,tr->ct/dot_general | solution.py:40
  16.2 0.0 collective-permute-done.3
  16.2 0.0 copy-done.7
  16.3 0.1 pad_add_fusion
  16.3 0.1 slice_compare_fusion
  16.4 0.1 iota_select_fusion
  16.5 10.7 %collective-permute-done = bf16[512,1024]{1,0:T(8,128)(2,1)} collective-permute-done((bf16[512,1024]{1,0:T(8,128)(2,1)}, bf16[512,1024]{1,0:T(8,128)(2,1)}, u32[]{:S(2)}, u32[]{:S(2)}) %collective-permute-start) | collective-permute-done | bytes 1048608 | tf_op jit(solution)/shard_map/ppermute | solution.py:47
  27.1 2.2 %collective-permute-start.1 = (bf16[512,1024]{1,0:T(8,128)(2,1)}, bf16[512,1024]{1,0:T(8,128)(2,1)S(1)}, u32[]{:S(2)}, u32[]{:S(2)}) collective-permute-start(bf16[512,1024]{1,0:T(8,128)(2,1)} %collective-permute-done), channel_id=1, source_target_pairs={{0,3},{1,0},{2,1},{3,2},{4,7},{5,4},{6,5},{7,6},{8,11},{9,8},{10,9... | collective-permute-start | bytes 3145736 | tf_op jit(solution)/shard_map/ppermute | solution.py:47
  29.3 0.3 reduce-window.9
  29.6 0.1 slice.278
  29.7 0.1 slice_reduce_fusion
  29.8 0.1 maximum_bitcast_fusion
  29.9 0.1 add_compare_fusion.29
  30.0 0.1 add_compare_fusion.20
  30.1 0.1 add_compare_fusion.11
  30.2 26.0 %collective-permute-done.1 = bf16[512,1024]{1,0:T(8,128)(2,1)S(1)} collective-permute-done((bf16[512,1024]{1,0:T(8,128)(2,1)}, bf16[512,1024]{1,0:T(8,128)(2,1)S(1)}, u32[]{:S(2)}, u32[]{:S(2)}) %collective-permute-start.1) | collective-permute-done | bytes 1048608 | tf_op jit(solution)/shard_map/ppermute | solution.py:47
  56.1 1.8 %collective-permute-start.2 = (bf16[512,1024]{1,0:T(8,128)(2,1)S(1)}, bf16[512,1024]{1,0:T(8,128)(2,1)}, u32[]{:S(2)}, u32[]{:S(2)}) collective-permute-start(bf16[512,1024]{1,0:T(8,128)(2,1)S(1)} %collective-permute-done.1), channel_id=1, source_target_pairs={{0,3},{1,0},{2,1},{3,2},{4,7},{5,4},{6,5},{7,6},{8,11},{9,8},{10,9... | collective-permute-start | bytes 3145736 | tf_op jit(solution)/shard_map/ppermute | solution.py:47
  57.9 3.3 %fusion.53 = f32[512,1024]{1,0:T(8,128)} fusion(bf16[512,1024]{1,0:T(8,128)(2,1)} %collective-permute-done, bf16[1,512,2048]{2,1,0:T(8,128)(2,1)S(1)} %copy-done, s32[]{:T(128)S(6)} %select_n.124), kind=kOutput, calls=%fused_computation.92 | convolution fusion | flops 536870912 | bytes 3670020 | tf_op jit(solution)/shard_map/rc,tr->ct/dot_general | solution.py:48
  61.2 2.0 %fusion.51 = f32[512,1024]{1,0:T(8,128)} fusion(bf16[512,1024]{1,0:T(8,128)(2,1)S(1)} %collective-permute-done.1, bf16[1,512,2048]{2,1,0:T(8,128)(2,1)S(1)} %copy-done, s32[]{:T(128)S(6)} %select_n.126), kind=kOutput, calls=%fused_computation.90 | convolution fusion | flops 536870912 | bytes 3670020 | tf_op jit(solution)/shard_map/rc,tr->ct/dot_general | solution.py:48
  63.3 5.1 %fusion.12 = f32[1024,512]{0,1:T(8,128)S(1)} fusion(bf16[2048,1024]{1,0:T(8,128)(2,1)} %all-gather.3.cloned.1.call-done, bf16[1,512,2048]{2,1,0:T(8,128)(2,1)S(1)} %copy-done), kind=kOutput, calls=%fused_computation.44 | convolution fusion | flops 2147483648 | bytes 8388608 | tf_op jit(solution)/shard_map/rc,tr->ct/dot_general | solution.py:57
  68.4 0.0 copy-start.6
  68.4 11.3 %collective-permute-done.2 = bf16[512,1024]{1,0:T(8,128)(2,1)} collective-permute-done((bf16[512,1024]{1,0:T(8,128)(2,1)S(1)}, bf16[512,1024]{1,0:T(8,128)(2,1)}, u32[]{:S(2)}, u32[]{:S(2)}) %collective-permute-start.2) | collective-permute-done | bytes 1048608 | tf_op jit(solution)/shard_map/ppermute | solution.py:47
  79.7 0.0 copy-done.1
  79.7 0.0 copy-done.2
  79.7 0.0 copy-done.3
  79.7 2.3 %fusion.14 = bf16[1024,512]{0,1:T(8,128)(2,1)S(1)} fusion(f32[1024,512]{0,1:T(8,128)S(1)} %fusion.12, f32[512,1024]{1,0:T(8,128)S(1)} %copy-done.3, f32[512,1024]{1,0:T(8,128)S(1)} %copy-done.1, f32[512,1024]{1,0:T(8,128)S(1)} %copy-done.2, bf16[512,1024]{1,0:T(8,128)(2,1)} %collective-permute-done.2, bf16[1,512,2048]{2,1,0:T(8,128)(2,1)S(1)} %copy-done, ...), kind=kOutput, calls=%fused_computation.47 | convolution fusion | flops 541065216 | bytes 11010052 | tf_op jit(solution)/shard_map/rc,tr->ct/dot_general | solution.py:48
  82.1 2.9 %collective-permute-start.4 = (bf16[1024,30]{0,1:T(8,128)(2,1)S(1)}, bf16[1024,30]{0,1:T(8,128)(2,1)S(1)}, u32[]{:S(2)}, u32[]{:S(2)}) collective-permute-start(bf16[1024,30]{0,1:T(8,128)(2,1)S(1)} %slice.341), channel_id=1, source_target_pairs={{0,4},{4,8},{8,12},{12,16},{16,20},{20,24},{24,28},{1,5},{5,9},{9,... | collective-permute-start | bytes 184328 | tf_op jit(solution)/shard_map/ppermute | solution.py:12
  85.0 0.1 add_compare_fusion.2
  85.1 1.8 %collective-permute-done.4 = bf16[1024,30]{0,1:T(8,128)(2,1)S(1)} collective-permute-done((bf16[1024,30]{0,1:T(8,128)(2,1)S(1)}, bf16[1024,30]{0,1:T(8,128)(2,1)S(1)}, u32[]{:S(2)}, u32[]{:S(2)}) %collective-permute-start.4) | collective-permute-done | bytes 61472 | tf_op jit(solution)/shard_map/ppermute | solution.py:12
  86.9 0.0 copy-done.6
  86.9 15.9 %add_convert_fusion = bf16[1024,512]{0,1:T(8,128)(2,1)S(1)} fusion(bf16[1024,512]{0,1:T(8,128)(2,1)S(1)} %fusion.14, bf16[1024,30]{0,1:T(8,128)(2,1)S(1)} %collective-permute-done.4, f32[1024]{0:T(1024)S(1)} %bitcast.75, f32[1024]{0:T(1024)S(1)} %bitcast.76, f32[1024]{0:T(1024)S(1)} %bitcast.78, f32[1024]{0:T(1024)S(1)} %bitcast.79, f32[1024]{0:T(1024)S(1)} %bitcast.80, ...), kind=kLoop, calls=%fused_computation.48 | loop fusion | flops 112197632 | bytes 2305024 | tf_op jit(solution)/shard_map/convert_element_type | solution.py:68
  102.8 0.2 convert_reduce_fusion
  103.1 0.4 fusion.3
  103.5 0.0 all-gather.5.cloned.1.call-done
  103.5 6.3 %fusion = bf16[1,512,2048]{2,1,0:T(8,128)(2,1)} fusion(bf16[1024,2048]{1,0:T(8,128)(2,1)} %all-gather.5.cloned.1.call-done, bf16[1024,512]{0,1:T(8,128)(2,1)S(1)} %add_convert_fusion, f32[1024]{0:T(1024)S(1)} %copy-done.8, f32[1024]{0:T(1024)S(1)} %copy-done.9, f32[512]{0:T(512)S(1)} %add_rsqrt_fusion, f32[512]{0:T(512)S(1)} %broadcast_multiply_fusion), kind=kOutput, calls=%fused_computation.30 | convolution fusion | flops 2153775104 | bytes 7352320 | tf_op jit(solution)/shard_map/ct,cr->tr/dot_general | solution.py:74
  (17 shorter events, 0.1 us)
Async XLA Ops:
  6.5 7.6 %copy-start = (bf16[1,512,2048]{2,1,0:T(8,128)(2,1)S(1)}, bf16[1,512,2048]{2,1,0:T(8,128)(2,1)}, u32[]{:S(2)}) copy-start(bf16[1,512,2048]{2,1,0:T(8,128)(2,1)} %param.9) | copy-start | bytes 6291460
  6.5 7.6 %copy-start.4 = (bf16[512,1024]{1,0:T(8,128)(2,1)S(1)}, bf16[512,1024]{1,0:T(8,128)(2,1)}, u32[]{:S(2)}) copy-start(bf16[512,1024]{1,0:T(8,128)(2,1)} %param.11) | copy-start | bytes 3145732
  6.5 7.4 %copy-start.5 = (f32[31,1024]{1,0:T(8,128)S(1)}, f32[31,1024]{1,0:T(8,128)}, u32[]{:S(2)}) copy-start(f32[31,1024]{1,0:T(8,128)} %param.14) | copy-start | bytes 380932
  6.5 56.7 %all-gather.3.cloned.1.call-start = ((), (), s32[]{:S(2)}) async-start(), calls=%async_computation | async-start | bytes 5242880 | tf_op jit(solution)/shard_map/all_gather | solution.py:59
  7.3 96.2 %all-gather.5.cloned.1.call-start = ((), (), s32[]{:S(2)}) async-start(), calls=%async_computation.1 | async-start | bytes 5242880 | tf_op jit(solution)/shard_map/all_gather | solution.py:77
  7.3 19.8 %collective-permute-start = (bf16[512,1024]{1,0:T(8,128)(2,1)}, bf16[512,1024]{1,0:T(8,128)(2,1)}, u32[]{:S(2)}, u32[]{:S(2)}) collective-permute-start(bf16[512,1024]{1,0:T(8,128)(2,1)} %param.11), channel_id=1, source_target_pairs={{0,3},{1,0},{2,1},{3,2},{4,7},{5,4},{6,5},{7,6},{8,11},{9,8},{10,9... | collective-permute-start | bytes 3145736 | tf_op jit(solution)/shard_map/ppermute | solution.py:47
  10.5 5.7 %collective-permute-start.3 = (s32[30]{0:T(128)S(1)}, s32[30]{0:T(128)S(1)}, u32[]{:S(2)}, u32[]{:S(2)}) collective-permute-start(s32[30]{0:T(128)S(1)} %slice_bitcast_fusion), channel_id=1, source_target_pairs={{0,4},{4,8},{8,12},{12,16},{16,20},{20,24},{24,28},{1,5},{5,9},{9,... | collective-permute-start | bytes 368 | tf_op jit(solution)/shard_map/ppermute | solution.py:12
  13.9 2.3 %copy-start.7 = (s32[1,512]{1,0:T(1,128)S(1)}, s32[1,512]{1,0:T(1,128)}, u32[]{:S(2)}) copy-start(s32[1,512]{1,0:T(1,128)} %param.10) | copy-start | bytes 6148
  27.1 29.0 %collective-permute-start.1 = (bf16[512,1024]{1,0:T(8,128)(2,1)}, bf16[512,1024]{1,0:T(8,128)(2,1)S(1)}, u32[]{:S(2)}, u32[]{:S(2)}) collective-permute-start(bf16[512,1024]{1,0:T(8,128)(2,1)} %collective-permute-done), channel_id=1, source_target_pairs={{0,3},{1,0},{2,1},{3,2},{4,7},{5,4},{6,5},{7,6},{8,11},{9,8},{10,9... | collective-permute-start | bytes 3145736 | tf_op jit(solution)/shard_map/ppermute | solution.py:47
  56.1 23.6 %collective-permute-start.2 = (bf16[512,1024]{1,0:T(8,128)(2,1)S(1)}, bf16[512,1024]{1,0:T(8,128)(2,1)}, u32[]{:S(2)}, u32[]{:S(2)}) collective-permute-start(bf16[512,1024]{1,0:T(8,128)(2,1)S(1)} %collective-permute-done.1), channel_id=1, source_target_pairs={{0,3},{1,0},{2,1},{3,2},{4,7},{5,4},{6,5},{7,6},{8,11},{9,8},{10,9... | collective-permute-start | bytes 3145736 | tf_op jit(solution)/shard_map/ppermute | solution.py:47
  63.2 16.5 %copy-start.1 = (f32[512,1024]{1,0:T(8,128)S(1)}, f32[512,1024]{1,0:T(8,128)}, u32[]{:S(2)}) copy-start(f32[512,1024]{1,0:T(8,128)} %fusion.55) | copy-start | bytes 6291460
  63.2 16.5 %copy-start.2 = (f32[512,1024]{1,0:T(8,128)S(1)}, f32[512,1024]{1,0:T(8,128)}, u32[]{:S(2)}) copy-start(f32[512,1024]{1,0:T(8,128)} %fusion.53) | copy-start | bytes 6291460
  63.2 16.5 %copy-start.3 = (f32[512,1024]{1,0:T(8,128)S(1)}, f32[512,1024]{1,0:T(8,128)}, u32[]{:S(2)}) copy-start(f32[512,1024]{1,0:T(8,128)} %fusion.51) | copy-start | bytes 6291460
  68.4 18.5 %copy-start.6 = (f32[1024]{0:T(1024)S(1)}, f32[1024]{0:T(1024)}, u32[]{:S(2)}) copy-start(f32[1024]{0:T(1024)} %param.15) | copy-start | bytes 12292
  82.1 4.8 %collective-permute-start.4 = (bf16[1024,30]{0,1:T(8,128)(2,1)S(1)}, bf16[1024,30]{0,1:T(8,128)(2,1)S(1)}, u32[]{:S(2)}, u32[]{:S(2)}) collective-permute-start(bf16[1024,30]{0,1:T(8,128)(2,1)S(1)} %slice.341), channel_id=1, source_target_pairs={{0,4},{4,8},{8,12},{12,16},{16,20},{20,24},{24,28},{1,5},{5,9},{9,... | collective-permute-start | bytes 184328 | tf_op jit(solution)/shard_map/ppermute | solution.py:12
  86.9 16.6 %copy-start.8 = (f32[1024]{0:T(1024)S(1)}, f32[1024]{0:T(1024)}, u32[]{:S(2)}) copy-start(f32[1024]{0:T(1024)} %param.17) | copy-start | bytes 12292
  86.9 16.6 %copy-start.9 = (f32[1024]{0:T(1024)S(1)}, f32[1024]{0:T(1024)}, u32[]{:S(2)}) copy-start(f32[1024]{0:T(1024)} %param.16) | copy-start | bytes 12292
Sparse Core Ops, SparseCore 0:
  8.9 46.7 all-gather.2
  57.2 38.0 all-gather.4
